TPU v7x, 32 devices: a whole 2x2x4 slice. The times are simulated.
32 devices in a mesh: sp: 8 (over z, x), tp: 4 (over y, core).
Axes of the slice: x: 2, y: 2, z: 4, core: 2. Of those that a mesh axis runs over, the one named last changes fastest.
Arguments:
- mixed: bfloat16 [1024, 2048], P('sp'), may hold values from -6 to 6
- cotangent: bfloat16 [1024, 2048], P('sp'), may hold values from -6 to 6
- routes: int32 [1024, 2], P('sp'), may hold values from 0 to 7, all different within a row; in each aligned block of 128 rows (0 to 127, 128 to 255, ...) at most 64 rows name the same one
- gates: float32 [1024, 2], P('sp'), may hold values from 0.1 to 1
- w_gate: bfloat16 [8, 2048, 1024], P('sp', None, 'tp'), may hold values from -0.125 to 0.125
- w_up: bfloat16 [8, 2048, 1024], P('sp', None, 'tp'), may hold values from -0.125 to 0.125
- w_down: bfloat16 [8, 1024, 2048], P('sp', 'tp'), may hold values from -0.1875 to 0.1875
- out_weight: bfloat16 [1024, 2048], P('tp'), may hold values from -0.1875 to 0.1875
- gate_pre: bfloat16 [1024, 1024], P('sp', 'tp'), may hold values from -8 to 8
- mixer_out: bfloat16 [1024, 1024], P('sp', 'tp'), may hold values from -6 to 6
- values: bfloat16 [1024, 1024], P('sp', 'tp'), may hold values from -6 to 6
- write_keys: bfloat16 [1024, 512], P('sp', 'tp'), may hold values from -1.25 to 1.25
- read_keys: bfloat16 [1024, 512], P('sp', 'tp'), may hold values from -1.25 to 1.25
- log_decay: float32 [16, 1024], P('tp', 'sp'), may hold values from -0.08 to 0
- entry_states: float32 [8, 16, 64, 128], P('sp', 'tp'), may hold values from -6 to 6
Outputs:
- d_w_gate: bfloat16 [8, 2048, 1024], P('sp', None, 'tp')
- d_w_up: bfloat16 [8, 2048, 1024], P('sp', None, 'tp')
- d_w_down: bfloat16 [8, 1024, 2048], P('sp', 'tp')
- d_out_weight: float32 [2048, 1024], P('sp', 'tp')
- d_input: bfloat16 [1024, 2048], P('sp', 'tp')
- d_values: bfloat16 [1024, 1024], P('sp', 'tp')
- d_write: float32 [1024, 512], P('sp', 'tp')
- d_read: float32 [1024, 512], P('sp', 'tp')
- d_gate: bfloat16 [1024, 1024], P('sp', 'tp')
Inputs may be any that keep to these rules, and one draw needn't show every extreme that they name: `routes`: each row names 2 different experts; in the 128 rows of one device no expert is named more than 64 times, and in some blocks one is named exactly 64 times.
All inputs are finite; a program needn't handle non-finite values.
Results may differ from a plain program's by a relative error of at most 0.0062.
Values may be sent and summed in bfloat16 or wider, within the bound.
A program may use at most 64 MiB of HBM per device.

v0:
```python
import jax
import jax.numpy as jnp
from jax import lax
from jax.sharding import PartitionSpec as P

D = 2048
HEAD_DIM = 64
BLOCK = 128
TOPK = 2
TOK_DEV = 128
precise = lax.Precision.HIGHEST


def prefix(part, axis, combine, identity):
    count = lax.axis_size(axis)
    place = lax.axis_index(axis)
    ahead = count - 1 - place
    gathered = jax.tree.map(lambda a: lax.all_gather(a, axis), part)
    state = jax.tree.map(lambda a, e: jnp.zeros_like(a) + jnp.asarray(e, a.dtype), part, identity)

    def one(lap, state):
        source = count - 1 - lap
        return combine(
            state, jax.tree.map(lambda a: lax.dynamic_index_in_dim(a, source, 0, False), gathered)
        )

    return lax.fori_loop(0, ahead, one, state)


def silu_grad(pre_act):
    logistic = jax.nn.sigmoid(pre_act)
    return logistic * (1.0 + pre_act * (1.0 - logistic))


def contract_rows(first_op, second_op):
    return lax.dot_general(
        first_op, second_op, (((0,), (0,)), ((), ())), preferred_element_type=jnp.float32
    )


def contract_cols(first_op, second_op):
    return lax.dot_general(
        first_op, second_op, (((1,), (1,)), ((), ())), preferred_element_type=jnp.float32
    )


def combine_state(earlier, later):
    return (later[0] * earlier[0], later[1] + later[0][:, None, None] * earlier[1])


def block_back(grad_state, inputs_x, grad_y, log_rate, write_rows, read_rows, start_state):
    block_len = log_rate.shape[0]
    running = jnp.cumsum(log_rate, axis=0)
    causal_mask = (jnp.arange(block_len)[:, None] >= jnp.arange(block_len)[None, :])[:, :, None]
    spread = running[:, None, :] - running[None, :, :]
    decay_mat = jnp.where(causal_mask, jnp.exp(jnp.where(causal_mask, spread, 0.0)), 0.0)
    intersection = jnp.dot(read_rows, write_rows.T, precision=precise)
    mixing = intersection[:, :, None] * decay_mat
    to_end = jnp.exp(running[-1][None, :] - running)
    from_start = jnp.exp(running)
    grad_x = jnp.einsum("lsj,ljp->sjp", mixing, grad_y, precision=precise) + to_end[
        :, :, None
    ] * jnp.einsum("sn,jpn->sjp", write_rows, grad_state, precision=precise)
    weighted = jnp.einsum("ljp,sjp->lsj", grad_y, inputs_x, precision=precise) * decay_mat
    grad_w = jnp.einsum("lsj,ln->sn", weighted, read_rows, precision=precise) + jnp.einsum(
        "sj,sjp,jpn->sn", to_end, inputs_x, grad_state, precision=precise
    )
    grad_r = jnp.einsum("lsj,sn->ln", weighted, write_rows, precision=precise) + jnp.einsum(
        "lj,ljp,jpn->ln", from_start, grad_y, start_state, precision=precise
    )
    earlier = jnp.exp(running[-1])[:, None, None] * grad_state + jnp.einsum(
        "lj,ljp,ln->jpn", from_start, grad_y, read_rows, precision=precise
    )
    return (earlier, grad_x, grad_w, grad_r)


def body(
    mixed,
    cotangent,
    routes,
    gates,
    w_gate,
    w_up,
    w_down,
    out_weight,
    gate_pre,
    mixer_out,
    values,
    write_keys,
    read_keys,
    log_decay,
    entry_states,
):
    sp_count = lax.axis_size("sp")
    tp_count = lax.axis_size("tp")
    capacity = 4 * TOK_DEV // sp_count
    assigned = TOK_DEV * TOPK
    picks = routes.reshape(assigned)
    onehot = (picks[:, None] == jnp.arange(sp_count, dtype=jnp.int32)[None, :]).astype(jnp.int32)
    earlier_same = jnp.cumsum(onehot, axis=0) - onehot
    slot_of = jnp.sum(earlier_same * onehot, axis=1)
    target = picks * capacity + slot_of
    anchor = (
        jnp.full((sp_count * capacity,), assigned, jnp.int32)
        .at[target]
        .set(jnp.arange(assigned, dtype=jnp.int32))
    )
    weight_g = w_gate[0]
    weight_u = w_up[0]
    weight_d = w_down[0]
    column_count = D // tp_count
    offset = lax.axis_index("tp") * column_count
    tok_slice = lax.dynamic_slice_in_dim(mixed, offset, column_count, 1)
    cot_slice = lax.dynamic_slice_in_dim(cotangent, offset, column_count, 1)
    columns = tok_slice.shape[1]
    scaled = (
        (gates[:, :, None] * cot_slice[:, None, :].astype(jnp.float32))
        .astype(jnp.bfloat16)
        .reshape(assigned, columns)
    )
    empty_row = jnp.zeros((1, columns), jnp.bfloat16)
    cot_buffer = jnp.concatenate([scaled, empty_row])[anchor].reshape(sp_count, capacity, columns)
    tok_buffer = jnp.concatenate([tok_slice, empty_row])[anchor // TOPK].reshape(
        sp_count, capacity, columns
    )
    tok_buffer, cot_buffer = (tok_buffer, cot_buffer)
    tok_part, cot_part = (
        lax.all_to_all(tok_buffer, "sp", split_axis=0, concat_axis=0, tiled=True),
        lax.all_to_all(cot_buffer, "sp", split_axis=0, concat_axis=0, tiled=True),
    )
    tok_rows, cot_rows = (
        lax.all_gather(tok_part, "tp", axis=2, tiled=True),
        lax.all_gather(cot_part, "tp", axis=2, tiled=True),
    )
    expert_tok_rows = tok_rows
    expert_cot_rows = cot_rows
    expert_tok_rows = expert_tok_rows.reshape(-1, D)
    expert_cot_rows = expert_cot_rows.reshape(-1, D)
    pre_gate = jnp.dot(expert_tok_rows, weight_g, preferred_element_type=jnp.float32)
    pre_up = jnp.dot(expert_tok_rows, weight_u, preferred_element_type=jnp.float32)
    active = jax.nn.silu(pre_gate)
    hidden = (active * pre_up).astype(jnp.bfloat16)
    grad_down = contract_rows(hidden, expert_cot_rows)
    grad_hidden = contract_cols(expert_cot_rows, weight_d)
    grad_gate = (grad_hidden * pre_up * silu_grad(pre_gate)).astype(jnp.bfloat16)
    grad_upval = (grad_hidden * active).astype(jnp.bfloat16)
    grad_wg = contract_rows(expert_tok_rows, grad_gate)
    grad_wu = contract_rows(expert_tok_rows, grad_upval)
    partial_value = contract_cols(grad_gate, weight_g) + contract_cols(grad_upval, weight_u)
    grad_wg, grad_wu, grad_down, partial_value = (grad_wg, grad_wu, grad_down, partial_value)
    row_total = partial_value.shape[0]
    pieces = partial_value.astype(jnp.bfloat16).reshape(row_total, tp_count, column_count)
    received = lax.all_to_all(pieces, "tp", split_axis=1, concat_axis=1, tiled=True)
    summed = (
        jnp.sum(received.astype(jnp.float32), axis=1)
        .astype(jnp.bfloat16)
        .reshape(sp_count, capacity, column_count)
    )
    returned = lax.all_to_all(summed, "sp", split_axis=0, concat_axis=0, tiled=True)
    columns = returned.shape[-1]
    picked = returned.reshape(sp_count * capacity, columns)[target].reshape(TOK_DEV, TOPK, columns)
    d_input = (cot_slice.astype(jnp.float32) + jnp.sum(picked.astype(jnp.float32), axis=1)).astype(
        jnp.bfloat16
    )
    whole = lax.all_gather(d_input, "tp", axis=1, tiled=True)
    back_proj = contract_cols(whole, out_weight)
    pre_act = gate_pre.astype(jnp.float32)
    gate_act = jax.nn.silu(pre_act)
    saved_out = mixer_out.astype(jnp.float32)
    d_gate = (back_proj * saved_out * silu_grad(pre_act)).astype(jnp.bfloat16)
    gated = (saved_out * gate_act).astype(jnp.bfloat16)
    d_out_weight = lax.psum_scatter(
        contract_rows(whole, gated), "sp", scatter_dimension=0, tiled=True
    )
    head_count = out_weight.shape[0] // HEAD_DIM
    grad_y = (back_proj * gate_act).reshape(TOK_DEV, head_count, HEAD_DIM)
    inputs_x = values.astype(jnp.float32).reshape(TOK_DEV, head_count, HEAD_DIM)
    write_rows = write_keys.astype(jnp.float32)
    read_rows = read_keys.astype(jnp.float32)
    log_rate = log_decay.T
    total_run = jnp.cumsum(log_rate, axis=0)
    shard_decay = jnp.exp(total_run[-1])
    shard_grad = jnp.einsum(
        "lj,ljp,ln->jpn", jnp.exp(total_run), grad_y, read_rows, precision=precise
    )
    identity = (jnp.ones_like(shard_decay), jnp.zeros_like(shard_grad))
    incoming = prefix((shard_decay, shard_grad), "sp", combine_state, identity)
    grad_state = incoming[1]
    pieces_x = []
    pieces_w = []
    pieces_r = []
    for block_id in reversed(range(TOK_DEV // BLOCK)):
        grad_state, grad_x, grad_w, grad_r = block_back(
            grad_state, inputs_x, grad_y, log_rate, write_rows, read_rows, entry_states[block_id]
        )
        pieces_x.insert(0, grad_x)
        pieces_w.insert(0, grad_w)
        pieces_r.insert(0, grad_r)
    d_values = pieces_x[0].reshape(TOK_DEV, head_count * HEAD_DIM).astype(jnp.bfloat16)
    d_write = pieces_w[0]
    d_read = pieces_r[0]
    return (
        grad_wg.astype(jnp.bfloat16)[None],
        grad_wu.astype(jnp.bfloat16)[None],
        grad_down.astype(jnp.bfloat16)[None],
        d_out_weight,
        d_input,
        d_values,
        d_write,
        d_read,
        d_gate,
    )


def solution(mesh):
    return jax.shard_map(
        body,
        mesh=mesh,
        in_specs=(
            P("sp", None),
            P("sp", None),
            P("sp", None),
            P("sp", None),
            P("sp", None, "tp"),
            P("sp", None, "tp"),
            P("sp", "tp", None),
            P("tp", None),
            P("sp", "tp"),
            P("sp", "tp"),
            P("sp", "tp"),
            P("sp", "tp"),
            P("sp", "tp"),
            P("tp", "sp"),
            P("sp", "tp", None, None),
        ),
        out_specs=(
            P("sp", None, "tp"),
            P("sp", None, "tp"),
            P("sp", "tp", None),
            P("sp", "tp"),
            P("sp", "tp"),
            P("sp", "tp"),
            P("sp", "tp"),
            P("sp", "tp"),
            P("sp", "tp"),
        ),
        check_vma=False,
    )
```

profile of v0, /device:TPU:0, one launch (start us, length us, event | category | flops | bytes accessed | tf_op | source)
XLA Modules:
  0.0 265.6 jit_solution(14270438159502153664)
XLA Ops:
  7.2 0.8 broadcast_multiply_fusion
  8.0 0.8 copy.51
  8.8 0.1 eq.29
  8.9 0.1 eq.25
  9.1 0.1 copy.50
  9.2 0.1 mul.130
  9.3 0.6 reduce-window.6
  9.9 0.2 slice_reduce_fusion
  10.3 1.4 scatter_custom_fusion
  11.7 1.0 dynamic-slice_convert_fusion
  12.8 2.0 gather_fusion
  14.8 21.7 %all_to_all.20 = bf16[8,64,512]{2,1,0:T(8,128)(2,1)} all-to-all(bf16[8,64,512]{2,1,0:T(8,128)(2,1)S(1)} %bitcast.115), channel_id=1, replica_groups=mesh['sp'=8,'tp'=4] {'sp'}, dimensions={0} | all-to-all | bytes 1048576 | tf_op jit(solution)/shard_map/all_to_all | solution.py:128
  36.5 0.2 mul.134
  36.7 0.4 mul.135
  37.2 0.1 mul.132
  37.5 2.0 gather_fusion.1
  39.5 17.6 %all_to_all.21 = bf16[8,64,512]{2,1,0:T(8,128)(2,1)} all-to-all(bf16[8,64,512]{2,1,0:T(8,128)(2,1)S(1)} %bitcast.116), channel_id=1, replica_groups=mesh['sp'=8,'tp'=4] {'sp'}, dimensions={0} | all-to-all | bytes 1048576 | tf_op jit(solution)/shard_map/all_to_all | solution.py:129
  57.1 1.1 all-gather.6.cloned.1.call-done
  58.3 2.5 fusion.10
  60.7 0.7 fusion.13
  61.5 20.9 %all-gather.8.cloned.1.call-done = bf16[8,64,2048]{2,1,0:T(8,128)(2,1)} async-done(((bf16[8,64,512]{2,1,0:T(8,128)(2,1)}), bf16[8,64,2048]{2,1,0:T(8,128)(2,1)}) %all-gather.8.cloned.1.call-update) | async-done | bytes 2097168 | tf_op jit(solution)/shard_map/all_gather | solution.py:133
  82.4 2.7 %multiply_convert_fusion.1 = (bf16[512,256]{1,0:T(8,128)(2,1)S(1)}, bf16[512,256]{1,0:T(8,128)(2,1)S(1)}) fusion(f32[512,256]{1,0:T(8,128)S(1)} %fusion.10, f32[512,256]{1,0:T(8,128)S(1)} %fusion.13, bf16[512,2048]{1,0:T(8,128)(2,1)} %bitcast.117, bf16[1,256,2048]{2,1,0:T(8,128)(2,1)} %param.23), kind=kOutput, calls=%fused_computation.36 | convolution fusion | flops 538574848 | bytes 4718592 | tf_op jit(solution)/shard_map/dot_general | solution.py:42
  85.1 0.7 fusion.8
  85.9 0.8 add_convert_fusion
  86.6 0.2 copy.68
  86.8 28.1 %all_to_all.22 = bf16[512,4,512]{2,0,1:T(8,128)(2,1)S(1)} all-to-all(bf16[512,4,512]{2,0,1:T(8,128)(2,1)S(1)} %bitcast.113), channel_id=1, replica_groups=mesh['sp'=8,'tp'=4] {'tp'}, dimensions={1} | all-to-all | bytes 4194304 | tf_op jit(solution)/shard_map/all_to_all | solution.py:153
  114.9 1.2 reduce_sum.47
  116.2 5.5 %all-to-all-start.3 = ((bf16[8,64,512]{2,1,0:T(8,128)(2,1)}), bf16[8,64,512]{2,1,0:T(8,128)(2,1)S(1)}, u32[]{:S(2)}, u32[]{:S(2)}) async-start(bf16[8,64,512]{2,1,0:T(8,128)(2,1)} %bitcast.119), calls=%async_computation.3 | async-start | bytes 1048576 | tf_op jit(solution)/shard_map/all_to_all | solution.py:159
  121.8 0.2 reduce_window_sum.29
  122.1 13.7 %all-to-all-done.3 = bf16[8,64,512]{2,1,0:T(8,128)(2,1)S(1)} async-done(((bf16[8,64,512]{2,1,0:T(8,128)(2,1)}), bf16[8,64,512]{2,1,0:T(8,128)(2,1)S(1)}, u32[]{:S(2)}, u32[]{:S(2)}) %all-to-all-start.3) | async-done | bytes 524320 | tf_op jit(solution)/shard_map/all_to_all | solution.py:159
  135.8 1.2 gather_fusion.2
  137.0 0.3 reshape.147
  137.3 0.6 reduce_sum.48
  138.0 0.9 add_convert_fusion.1
  138.9 6.5 %all_gather.21 = bf16[128,2048]{1,0:T(8,128)(2,1)S(1)} all-gather(bf16[128,512]{1,0:T(8,128)(2,1)S(1)} %add_convert_fusion.1), channel_id=1, replica_groups=mesh['sp'=8,'tp'=4] {'tp'}, dimensions={1}, use_global_device_ids=true | all-gather | bytes 655360 | tf_op jit(solution)/shard_map/all_gather | solution.py:165
  145.4 2.3 fusion.21
  147.9 0.9 fusion.36
  148.8 0.2 reduce-scatter.2.cloned.1.call-start
  149.0 1.8 fusion.39
  151.0 0.1 copy.63
  151.2 18.8 %all-gather.1 = f32[8,1,4]{2,1,0:T(1,128)S(1)} all-gather(f32[1,1,4]{2,1,0:T(1,128)S(1)} %get-tuple-element.153), channel_id=1, replica_groups=mesh['sp'=8,'tp'=4] {'sp'}, dimensions={0}, use_global_device_ids=true | all-gather | bytes 144 | tf_op jit(solution)/shard_map/all_gather | solution.py:18
  170.0 0.1 fusion.57
  170.2 3.5 %fusion = bf16[1,2048,256]{2,1,0:T(8,128)(2,1)} fusion(bf16[512,2048]{1,0:T(8,128)(2,1)} %bitcast.134, bf16[512,256]{1,0:T(8,128)(2,1)S(1)} %get-tuple-element.147), kind=kOutput, calls=%fused_computation.10 | convolution fusion | flops 537395200 | bytes 3407872 | tf_op jit(solution)/shard_map/dot_general | solution.py:36
  173.7 1.7 fusion.1
  175.4 0.4 copy-done.7
  175.9 1.8 fusion.2
  177.6 0.4 convolution_bitcast_fusion.3
  178.0 0.4 fusion.4
  178.4 0.8 convolution_add_fusion
  179.3 8.7 %all-gather.10.cloned.1.call-done = f32[32,64,128]{2,1,0:T(8,128)} async-done(((f32[4,64,128]{2,1,0:T(8,128)}), f32[32,64,128]{2,1,0:T(8,128)}) %all-gather.10.cloned.1.call-update) | async-done | bytes 1048592 | tf_op jit(solution)/shard_map/all_gather | solution.py:18
  188.0 7.2 %while.14 = (s32[]{:T(128)}, f32[4,64,128]{2,1,0:T(8,128)S(1)}, s32[]{:T(128)}, f32[8,4,64,128]{3,2,1,0:T(8,128)}, f32[8,4]{1,0:T(8,128)S(1)}, /*index=5*/s32[]{:T(128)}, s32[]{:T(128)}, s32[]{:T(128)}, s32[]{:T(128)}) while((s32[]{:T(128)}, f32[4,64,128]{2,1,0:T(8,128)S(1)}, s32[]{:T(128)}, f32[8,4,64,128]{3,2,1,0:T(8,128)}, ...), condition=%wide.region_9.10_spmd, body=%wide.region_8.9_spmd.sunk | while | flops 65542 | bytes 393419 | solution.py:27
  188.0 1.0 bitcast_add_fusion.2
  189.0 1.0 bitcast_add_fusion.2
  190.1 1.0 bitcast_add_fusion.2
  191.1 1.0 bitcast_add_fusion.2
  192.1 1.0 bitcast_add_fusion.2
  193.2 1.0 bitcast_add_fusion.2
  194.2 1.0 bitcast_add_fusion.2
  195.2 0.2 fusion.6
  195.5 0.5 fusion.7
  195.9 0.7 copy.64
  196.7 0.4 convolution_bitcast_fusion.4
  197.1 0.9 convolution_add_fusion.1
  198.0 61.1 %reduce-scatter.2.cloned.1.call-done = f32[256,256]{1,0:T(8,128)} async-done(((f32[2048,256]{1,0:T(8,128)}), f32[256,256]{1,0:T(8,128)}) %reduce-scatter.2.cloned.1.call-update) | async-done | bytes 262160 | tf_op jit(solution)/shard_map/reduce_scatter | solution.py:172
  (75 shorter events, 1.2 us)
Async XLA Ops:
  7.2 51.1 %copy-start = (bf16[1,2048,256]{2,1,0:T(8,128)(2,1)S(1)}, bf16[1,2048,256]{2,1,0:T(8,128)(2,1)}, u32[]{:S(2)}) copy-start(bf16[1,2048,256]{2,1,0:T(8,128)(2,1)} %param.21) | copy-start | bytes 3145732
  7.2 51.1 %all-gather.6.cloned.1.call-start = ((), (), s32[]{:S(2)}) async-start(), calls=%async_computation.5 | async-start | bytes 2621440 | tf_op jit(solution)/shard_map/all_gather | solution.py:132
  14.7 22.4 %copy-start.17 = (f32[128,2]{0,1:T(2,128)S(1)}, f32[128,2]{0,1:T(2,128)}, u32[]{:S(2)}) copy-start(f32[128,2]{0,1:T(2,128)} %param.20) | copy-start | bytes 3076
  36.5 45.9 %all-gather.8.cloned.1.call-start = ((), (), s32[]{:S(2)}) async-start(), calls=%async_computation.6 | async-start | bytes 2621440 | tf_op jit(solution)/shard_map/all_gather | solution.py:133
  57.1 3.6 %copy-start.2 = (bf16[1,2048,256]{2,1,0:T(8,128)(2,1)S(1)}, bf16[1,2048,256]{2,1,0:T(8,128)(2,1)}, u32[]{:S(2)}) copy-start(bf16[1,2048,256]{2,1,0:T(8,128)(2,1)} %param.22) | copy-start | bytes 3145732
  58.3 2.5 copy-start.18
  60.7 24.3 %copy-start.4 = (f32[512,256]{1,0:T(8,128)}, f32[512,256]{1,0:T(8,128)S(1)}, u32[]{:S(2)}) copy-start(f32[512,256]{1,0:T(8,128)S(1)} %fusion.10) | copy-start | bytes 1572868
  61.5 23.6 %copy-start.6 = (f32[512,256]{1,0:T(8,128)}, f32[512,256]{1,0:T(8,128)S(1)}, u32[]{:S(2)}) copy-start(f32[512,256]{1,0:T(8,128)S(1)} %fusion.13) | copy-start | bytes 1572868
  85.1 0.8 copy-start.10
  114.9 6.8 %copy-start.16 = (f32[4,128]{1,0:T(4,128)S(1)}, f32[4,128]{1,0:T(4,128)}, u32[]{:S(2)}) copy-start(f32[4,128]{1,0:T(4,128)} %param.30) | copy-start | bytes 6148
  116.2 19.7 %all-to-all-start.3 = ((bf16[8,64,512]{2,1,0:T(8,128)(2,1)}), bf16[8,64,512]{2,1,0:T(8,128)(2,1)S(1)}, u32[]{:S(2)}, u32[]{:S(2)}) async-start(bf16[8,64,512]{2,1,0:T(8,128)(2,1)} %bitcast.119), calls=%async_computation.3 | async-start | bytes 1048576 | tf_op jit(solution)/shard_map/all_to_all | solution.py:159
  121.7 66.3 %all-gather.10.cloned.1.call-start = ((), (), s32[]{:S(2)}) async-start(), calls=%async_computation.8 | async-start | bytes 1179648 | tf_op jit(solution)/shard_map/all_gather | solution.py:18
  135.8 9.6 %copy-start.13 = (bf16[128,256]{1,0:T(8,128)(2,1)S(1)}, bf16[128,256]{1,0:T(8,128)(2,1)}, u32[]{:S(2)}) copy-start(bf16[128,256]{1,0:T(8,128)(2,1)} %param.26) | copy-start | bytes 196612
  135.8 9.6 %copy-start.14 = (bf16[128,256]{1,0:T(8,128)(2,1)S(1)}, bf16[128,256]{1,0:T(8,128)(2,1)}, u32[]{:S(2)}) copy-start(bf16[128,256]{1,0:T(8,128)(2,1)} %param.25) | copy-start | bytes 196612
  137.3 10.5 %copy-start.9 = (bf16[128,128]{1,0:T(8,128)(2,1)S(1)}, bf16[128,128]{1,0:T(8,128)(2,1)}, u32[]{:S(2)}) copy-start(bf16[128,128]{1,0:T(8,128)(2,1)} %param.29) | copy-start | bytes 98308
  138.9 12.0 %copy-start.3 = (bf16[128,512]{1,0:T(8,128)(2,1)}, bf16[128,512]{1,0:T(8,128)(2,1)S(1)}, u32[]{:S(2)}) copy-start(bf16[128,512]{1,0:T(8,128)(2,1)S(1)} %add_convert_fusion.1) | copy-start | bytes 393220
  148.8 2.2 copy-start.15
  148.8 21.2 %copy-start.8 = (bf16[128,128]{1,0:T(8,128)(2,1)S(1)}, bf16[128,128]{1,0:T(8,128)(2,1)}, u32[]{:S(2)}) copy-start(bf16[128,128]{1,0:T(8,128)(2,1)} %param.28) | copy-start | bytes 98308
  148.8 110.2 %reduce-scatter.2.cloned.1.call-start = ((), (), s32[]{:S(2)}) async-start(), calls=%async_computation.7 | async-start | bytes 2359296 | tf_op jit(solution)/shard_map/reduce_scatter | solution.py:172
  170.2 3.5 %copy-start.11 = (bf16[512,256]{1,0:T(8,128)(2,1)S(1)}, bf16[512,256]{1,0:T(8,128)(2,1)}, u32[]{:S(2)}) copy-start(bf16[512,256]{1,0:T(8,128)(2,1)} %copy-done.10) | copy-start | bytes 786436
  170.2 3.5 %copy-start.19 = (bf16[8,64,2048]{2,1,0:T(8,128)(2,1)S(1)}, bf16[8,64,2048]{2,1,0:T(8,128)(2,1)}, u32[]{:S(2)}) copy-start(bf16[8,64,2048]{2,1,0:T(8,128)(2,1)} %all-gather.6.cloned.1.call-done) | copy-start | bytes 6291460
  173.7 1.8 copy-start.1
  173.7 1.8 copy-start.5
  173.7 2.2 copy-start.7
  175.9 1.8 copy-start.12
Sparse Core Ops, SparseCore 0:
  36.6 21.5 all-gather.5
  59.8 22.5 all-gather.7
  148.9 38.9 all-gather.9
  191.9 67.0 reduce-scatter.1
where the time goes:
time: 266 us
  waiting for transfers between devices  106 us (40%)
  blocking collectives  92.8 us (35%)
  matrix products  23.1 us (9%)
  between operations  14.2 us (5%)
  other arithmetic  12.6 us (5%)
  local copies, waits for them, and re-layouts  11.2 us (4%)
  starting transfers between devices  5.85 us (2%)
    reduce_scatter x1, waiting for transfers between devices, body(): lax.psum_scatter(contract_rows(whole, gated), 'sp', scatter_dimension=0,...  61.1 us
    all_to_all x1, blocking collectives, body(): lax.all_to_all(pieces, 'tp', split_axis=1, concat_axis=1, tiled=True)  28.1 us
    all_to_all x1, blocking collectives, body(): lax.all_to_all(tok_buffer, 'sp', split_axis=0, concat_axis=0, tiled=True)  21.7 us
    all_gather x1, waiting for transfers between devices, body(): lax.all_gather(cot_part, 'tp', axis=2, tiled=True)  20.9 us
    all_gather x1, blocking collectives, prefix(): gathered = jax.tree.map(lambda a: lax.all_gather(a, axis), part)  18.8 us
    all_to_all x1, blocking collectives, body(): lax.all_to_all(cot_buffer, 'sp', split_axis=0, concat_axis=0, tiled=True)  17.6 us
    all_to_all x1, waiting for transfers between devices, body(): lax.all_to_all(summed, 'sp', split_axis=0, concat_axis=0, tiled=True)  13.7 us
    dot_general x4, matrix products, contract_rows(): lax.dot_general(first_op, second_op, (((0,), (0,)), ((), ())), preferred_...  8.79 us
  transfers between devices with their start and end apart: 5, of which 5 were waited for; matrix products, arithmetic and copies ran while one was open for 10% of the time, Pallas kernels for 0%

commit v1 on v0

--- a/solution.py
+++ b/solution.py
@@ -150,7 +150,10 @@
     grad_wg, grad_wu, grad_down, partial_value = (grad_wg, grad_wu, grad_down, partial_value)
     row_total = partial_value.shape[0]
     pieces = partial_value.astype(jnp.bfloat16).reshape(row_total, tp_count, column_count)
-    received = lax.all_to_all(pieces, "tp", split_axis=1, concat_axis=1, tiled=True)
+    received = jnp.concatenate(
+        lax.all_to_all(jnp.stack(jnp.split(pieces, lax.axis_size("tp"), axis=1)), "tp", 0, 0),
+        axis=1,
+    )
     summed = (
         jnp.sum(received.astype(jnp.float32), axis=1)
         .astype(jnp.bfloat16)

time: 266 us -> 275 us (1.034)
  local copies, waits for them, and re-layouts: 11.2 us -> 17.9 us
    reshape x1, local copies, waits for them, and re-layouts: 0.16 us -> 3.31 us  [body(): partial_value.astype(jnp.bfloat16)]
    split x0 -> x1, local copies, waits for them, and re-layouts: none -> 3.05 us  [body(): jnp.split(pieces, lax.axis_size('tp'), axis=1)]
where the time goes in v1:
time: 275 us; the launch traced here: 274 us
  waiting for transfers between devices  106 us (39%)
  blocking collectives  92.8 us (34%)
  matrix products  24.4 us (9%)
  local copies, waits for them, and re-layouts  17.9 us (7%)
  between operations  14.2 us (5%)
  other arithmetic  12.9 us (5%)
  starting transfers between devices  5.85 us (2%)
    reduce_scatter x1, waiting for transfers between devices, body(): lax.psum_scatter(contract_rows(whole, gated), 'sp', scatter_dimension=0,...  61.1 us
    all_to_all x1, blocking collectives, body(): lax.all_to_all(jnp.stack(jnp.split(pieces, lax.axis_size('tp'), axis=1)),...  28.1 us
    all_to_all x1, blocking collectives, body(): lax.all_to_all(tok_buffer, 'sp', split_axis=0, concat_axis=0, tiled=True)  21.7 us
    all_gather x1, waiting for transfers between devices, body(): lax.all_gather(cot_part, 'tp', axis=2, tiled=True)  20.9 us
    all_gather x1, blocking collectives, prefix(): gathered = jax.tree.map(lambda a: lax.all_gather(a, axis), part)  18.8 us
    all_to_all x1, blocking collectives, body(): lax.all_to_all(cot_buffer, 'sp', split_axis=0, concat_axis=0, tiled=True)  17.6 us
    all_to_all x1, waiting for transfers between devices, body(): lax.all_to_all(summed, 'sp', split_axis=0, concat_axis=0, tiled=True)  13.5 us
    all_gather x1, waiting for transfers between devices, prefix(): gathered = jax.tree.map(lambda a: lax.all_gather(a, axis), part)  8.92 us
  transfers between devices with their start and end apart: 5, of which 5 were waited for; matrix products, arithmetic and copies ran while one was open for 10% of the time, Pallas kernels for 0%

profile of v1, /device:TPU:0, one launch (start us, length us, event | category | flops | bytes accessed | tf_op | source)
XLA Modules:
  0.0 273.9 jit_solution(17687718839020685538)
XLA Ops:
  7.2 0.8 broadcast_multiply_fusion
  8.0 0.8 copy.58
  8.9 0.1 eq.25
  9.2 0.1 mul.130
  9.3 0.6 reduce-window.6
  9.9 0.2 slice_reduce_fusion
  10.3 1.4 scatter_custom_fusion
  11.7 1.0 dynamic-slice_convert_fusion
  12.8 2.0 gather_fusion
  14.8 21.7 %all_to_all.20 = bf16[8,64,512]{2,1,0:T(8,128)(2,1)} all-to-all(bf16[8,64,512]{2,1,0:T(8,128)(2,1)S(1)} %bitcast.121), channel_id=1, replica_groups=mesh['sp'=8,'tp'=4] {'sp'}, dimensions={0} | all-to-all | bytes 1048576 | tf_op jit(solution)/shard_map/all_to_all | solution.py:128
  36.5 0.2 mul.134
  36.7 0.4 mul.135
  37.2 0.1 mul.132
  37.5 2.0 gather_fusion.1
  39.5 17.6 %all_to_all.21 = bf16[8,64,512]{2,1,0:T(8,128)(2,1)} all-to-all(bf16[8,64,512]{2,1,0:T(8,128)(2,1)S(1)} %bitcast.122), channel_id=1, replica_groups=mesh['sp'=8,'tp'=4] {'sp'}, dimensions={0} | all-to-all | bytes 1048576 | tf_op jit(solution)/shard_map/all_to_all | solution.py:129
  57.1 1.1 all-gather.6.cloned.1.call-done
  58.3 2.5 fusion.10
  60.7 0.7 fusion.13
  61.5 20.9 %all-gather.8.cloned.1.call-done = bf16[8,64,2048]{2,1,0:T(8,128)(2,1)} async-done(((bf16[8,64,512]{2,1,0:T(8,128)(2,1)}), bf16[8,64,2048]{2,1,0:T(8,128)(2,1)}) %all-gather.8.cloned.1.call-update) | async-done | bytes 2097168 | tf_op jit(solution)/shard_map/all_gather | solution.py:133
  82.4 2.7 multiply_convert_fusion.1
  85.1 0.7 fusion.8
  85.9 2.1 add_convert_fusion
  88.0 3.3 %reshape.144 = bf16[512,4,512]{2,1,0:T(4,128)(2,1)S(1)} reshape(bf16[512,2048]{1,0:T(8,128)(2,1)} %add_convert_fusion) | data formatting | bytes 4194304 | tf_op jit(solution)/shard_map/reshape | solution.py:152
  91.3 3.1 %fusion.57 = (bf16[512,1,512]{2,1,0:T(2,128)(2,1)S(1)}, bf16[512,1,512]{2,1,0:T(2,128)(2,1)S(1)}, bf16[512,1,512]{2,1,0:T(2,128)(2,1)S(1)}, bf16[512,1,512]{2,1,0:T(2,128)(2,1)S(1)}) fusion(bf16[512,4,512]{2,1,0:T(4,128)(2,1)S(1)} %reshape.144), kind=kLoop, calls=%fused_computation.111 | loop fusion | bytes 4194304 | tf_op jit(solution)/shard_map/split | solution.py:154
  94.9 0.3 pad_maximum_fusion
  95.1 28.1 %all_to_all.22 = bf16[4,512,1,512]{3,1,2,0:T(8,128)(2,1)S(1)} all-to-all(bf16[4,512,1,512]{3,1,2,0:T(8,128)(2,1)S(1)} %pad_maximum_fusion), channel_id=1, replica_groups=mesh['sp'=8,'tp'=4] {'tp'}, dimensions={0} | all-to-all | bytes 4194304 | tf_op jit(solution)/shard_map/all_to_all | solution.py:154
  123.3 1.2 reduce_sum.47
  124.5 5.5 %all-to-all-start.3 = ((bf16[8,64,512]{2,1,0:T(8,128)(2,1)}), bf16[8,64,512]{2,1,0:T(8,128)(2,1)S(1)}, u32[]{:S(2)}, u32[]{:S(2)}) async-start(bf16[8,64,512]{2,1,0:T(8,128)(2,1)} %bitcast.125), calls=%async_computation.3 | async-start | bytes 1048576 | tf_op jit(solution)/shard_map/all_to_all | solution.py:162
  130.0 0.2 all-gather.10.cloned.1.call-start
  130.4 0.2 reduce_window_sum.29
  130.6 13.5 %all-to-all-done.3 = bf16[8,64,512]{2,1,0:T(8,128)(2,1)S(1)} async-done(((bf16[8,64,512]{2,1,0:T(8,128)(2,1)}), bf16[8,64,512]{2,1,0:T(8,128)(2,1)S(1)}, u32[]{:S(2)}, u32[]{:S(2)}) %all-to-all-start.3) | async-done | bytes 524320 | tf_op jit(solution)/shard_map/all_to_all | solution.py:162
  144.2 1.2 gather_fusion.2
  145.3 0.3 reshape.149
  145.7 0.6 reduce_sum.48
  146.3 0.9 add_convert_fusion.1
  147.3 6.5 %all_gather.21 = bf16[128,2048]{1,0:T(8,128)(2,1)S(1)} all-gather(bf16[128,512]{1,0:T(8,128)(2,1)S(1)} %add_convert_fusion.1), channel_id=1, replica_groups=mesh['sp'=8,'tp'=4] {'tp'}, dimensions={1}, use_global_device_ids=true | all-gather | bytes 655360 | tf_op jit(solution)/shard_map/all_gather | solution.py:168
  153.8 2.4 fusion.21
  156.2 0.9 fusion.36
  157.2 1.8 fusion.39
  159.2 0.1 copy.73
  159.3 18.8 %all-gather.1 = f32[8,1,4]{2,1,0:T(1,128)S(1)} all-gather(f32[1,1,4]{2,1,0:T(1,128)S(1)} %get-tuple-element.157), channel_id=1, replica_groups=mesh['sp'=8,'tp'=4] {'sp'}, dimensions={0}, use_global_device_ids=true | all-gather | bytes 144 | tf_op jit(solution)/shard_map/all_gather | solution.py:18
  178.2 0.2 fusion.58
  178.4 3.5 %fusion = bf16[1,2048,256]{2,1,0:T(8,128)(2,1)} fusion(bf16[512,2048]{1,0:T(8,128)(2,1)} %bitcast.144, bf16[512,256]{1,0:T(8,128)(2,1)S(1)} %get-tuple-element.151), kind=kOutput, calls=%fused_computation.10 | convolution fusion | flops 537395200 | bytes 3407872 | tf_op jit(solution)/shard_map/dot_general | solution.py:36
  181.9 1.8 fusion.1
  183.6 0.4 copy-done.7
  184.0 1.8 fusion.2
  185.7 0.4 convolution_bitcast_fusion.3
  186.1 0.4 fusion.4
  186.6 0.8 convolution_add_fusion
  187.4 8.9 %all-gather.10.cloned.1.call-done = f32[32,64,128]{2,1,0:T(8,128)} async-done(((f32[4,64,128]{2,1,0:T(8,128)}), f32[32,64,128]{2,1,0:T(8,128)}) %all-gather.10.cloned.1.call-update) | async-done | bytes 1048592 | tf_op jit(solution)/shard_map/all_gather | solution.py:18
  196.3 7.2 %while.14 = (s32[]{:T(128)}, f32[4,64,128]{2,1,0:T(8,128)S(1)}, s32[]{:T(128)}, f32[8,4,64,128]{3,2,1,0:T(8,128)}, f32[8,4]{1,0:T(8,128)S(1)}, /*index=5*/s32[]{:T(128)}, s32[]{:T(128)}, s32[]{:T(128)}, s32[]{:T(128)}) while((s32[]{:T(128)}, f32[4,64,128]{2,1,0:T(8,128)S(1)}, s32[]{:T(128)}, f32[8,4,64,128]{3,2,1,0:T(8,128)}, ...), condition=%wide.region_9.10_spmd, body=%wide.region_8.9_spmd.sunk | while | flops 65542 | bytes 393419 | solution.py:27
  196.3 1.0 bitcast_add_fusion.2
  197.4 1.0 bitcast_add_fusion.2
  198.4 1.0 bitcast_add_fusion.2
  199.5 1.0 bitcast_add_fusion.2
  200.5 1.0 bitcast_add_fusion.2
  201.5 1.0 bitcast_add_fusion.2
  202.6 1.0 bitcast_add_fusion.2
  203.6 0.2 fusion.6
  203.8 0.5 fusion.7
  204.3 0.7 copy.74
  205.0 0.4 convolution_bitcast_fusion.4
  205.4 0.9 convolution_add_fusion.1
  206.3 61.1 %reduce-scatter.2.cloned.1.call-done = f32[256,256]{1,0:T(8,128)} async-done(((f32[2048,256]{1,0:T(8,128)}), f32[256,256]{1,0:T(8,128)}) %reduce-scatter.2.cloned.1.call-update) | async-done | bytes 262160 | tf_op jit(solution)/shard_map/reduce_scatter | solution.py:175
  (81 shorter events, 2.0 us)
Async XLA Ops:
  7.2 51.1 %copy-start = (bf16[1,2048,256]{2,1,0:T(8,128)(2,1)S(1)}, bf16[1,2048,256]{2,1,0:T(8,128)(2,1)}, u32[]{:S(2)}) copy-start(bf16[1,2048,256]{2,1,0:T(8,128)(2,1)} %param.21) | copy-start | bytes 3145732
  7.2 51.1 %all-gather.6.cloned.1.call-start = ((), (), s32[]{:S(2)}) async-start(), calls=%async_computation.5 | async-start | bytes 2621440 | tf_op jit(solution)/shard_map/all_gather | solution.py:132
  14.7 22.4 %copy-start.17 = (f32[128,2]{0,1:T(2,128)S(1)}, f32[128,2]{0,1:T(2,128)}, u32[]{:S(2)}) copy-start(f32[128,2]{0,1:T(2,128)} %param.20) | copy-start | bytes 3076
  36.5 45.9 %all-gather.8.cloned.1.call-start = ((), (), s32[]{:S(2)}) async-start(), calls=%async_computation.6 | async-start | bytes 2621440 | tf_op jit(solution)/shard_map/all_gather | solution.py:133
  57.1 3.6 %copy-start.2 = (bf16[1,2048,256]{2,1,0:T(8,128)(2,1)S(1)}, bf16[1,2048,256]{2,1,0:T(8,128)(2,1)}, u32[]{:S(2)}) copy-start(bf16[1,2048,256]{2,1,0:T(8,128)(2,1)} %param.22) | copy-start | bytes 3145732
  58.3 2.5 copy-start.18
  60.7 24.3 %copy-start.4 = (f32[512,256]{1,0:T(8,128)}, f32[512,256]{1,0:T(8,128)S(1)}, u32[]{:S(2)}) copy-start(f32[512,256]{1,0:T(8,128)S(1)} %fusion.10) | copy-start | bytes 1572868
  61.5 23.6 %copy-start.6 = (f32[512,256]{1,0:T(8,128)}, f32[512,256]{1,0:T(8,128)S(1)}, u32[]{:S(2)}) copy-start(f32[512,256]{1,0:T(8,128)S(1)} %fusion.13) | copy-start | bytes 1572868
  85.1 0.8 copy-start.10
  123.3 7.0 %copy-start.16 = (f32[4,128]{1,0:T(4,128)S(1)}, f32[4,128]{1,0:T(4,128)}, u32[]{:S(2)}) copy-start(f32[4,128]{1,0:T(4,128)} %param.30) | copy-start | bytes 6148
  124.5 19.7 %all-to-all-start.3 = ((bf16[8,64,512]{2,1,0:T(8,128)(2,1)}), bf16[8,64,512]{2,1,0:T(8,128)(2,1)S(1)}, u32[]{:S(2)}, u32[]{:S(2)}) async-start(bf16[8,64,512]{2,1,0:T(8,128)(2,1)} %bitcast.125), calls=%async_computation.3 | async-start | bytes 1048576 | tf_op jit(solution)/shard_map/all_to_all | solution.py:162
  130.0 66.3 %all-gather.10.cloned.1.call-start = ((), (), s32[]{:S(2)}) async-start(), calls=%async_computation.8 | async-start | bytes 1179648 | tf_op jit(solution)/shard_map/all_gather | solution.py:18
  144.2 9.6 %copy-start.13 = (bf16[128,256]{1,0:T(8,128)(2,1)S(1)}, bf16[128,256]{1,0:T(8,128)(2,1)}, u32[]{:S(2)}) copy-start(bf16[128,256]{1,0:T(8,128)(2,1)} %param.26) | copy-start | bytes 196612
  144.2 9.6 %copy-start.14 = (bf16[128,256]{1,0:T(8,128)(2,1)S(1)}, bf16[128,256]{1,0:T(8,128)(2,1)}, u32[]{:S(2)}) copy-start(bf16[128,256]{1,0:T(8,128)(2,1)} %param.25) | copy-start | bytes 196612
  145.7 10.5 %copy-start.9 = (bf16[128,128]{1,0:T(8,128)(2,1)S(1)}, bf16[128,128]{1,0:T(8,128)(2,1)}, u32[]{:S(2)}) copy-start(bf16[128,128]{1,0:T(8,128)(2,1)} %param.29) | copy-start | bytes 98308
  147.3 11.8 %copy-start.3 = (bf16[128,512]{1,0:T(8,128)(2,1)}, bf16[128,512]{1,0:T(8,128)(2,1)S(1)}, u32[]{:S(2)}) copy-start(bf16[128,512]{1,0:T(8,128)(2,1)S(1)} %add_convert_fusion.1) | copy-start | bytes 393220
  157.1 2.1 copy-start.15
  157.1 21.1 %copy-start.8 = (bf16[128,128]{1,0:T(8,128)(2,1)S(1)}, bf16[128,128]{1,0:T(8,128)(2,1)}, u32[]{:S(2)}) copy-start(bf16[128,128]{1,0:T(8,128)(2,1)} %param.28) | copy-start | bytes 98308
  157.2 110.2 %reduce-scatter.2.cloned.1.call-start = ((), (), s32[]{:S(2)}) async-start(), calls=%async_computation.7 | async-start | bytes 2359296 | tf_op jit(solution)/shard_map/reduce_scatter | solution.py:175
  178.4 3.5 %copy-start.11 = (bf16[512,256]{1,0:T(8,128)(2,1)S(1)}, bf16[512,256]{1,0:T(8,128)(2,1)}, u32[]{:S(2)}) copy-start(bf16[512,256]{1,0:T(8,128)(2,1)} %copy-done.10) | copy-start | bytes 786436
  178.4 3.5 %copy-start.19 = (bf16[8,64,2048]{2,1,0:T(8,128)(2,1)S(1)}, bf16[8,64,2048]{2,1,0:T(8,128)(2,1)}, u32[]{:S(2)}) copy-start(bf16[8,64,2048]{2,1,0:T(8,128)(2,1)} %all-gather.6.cloned.1.call-done) | copy-start | bytes 6291460
  181.8 1.8 copy-start.1
  181.8 1.8 copy-start.5
  181.9 2.1 copy-start.7
  184.0 1.8 copy-start.12
Sparse Core Ops, SparseCore 0:
  36.6 21.5 all-gather.5
  59.8 22.5 all-gather.7
  157.3 38.9 all-gather.9
  200.3 67.0 reduce-scatter.1
